TPU v7x, 32 devices: a whole 2x2x4 slice. The times are simulated.
32 devices in a mesh: tp: 8 (over z, y), dp: 4 (over x, core).
Axes of the slice: x: 2, y: 2, z: 4, core: 2. Of those that a mesh axis runs over, the one named last changes fastest.
Arguments:
- hidden: bfloat16 [96, 4096], P(None, 'dp'), may hold values from -14 to 14
- lengths: int32 [96], P('dp'), may hold values from 1 to 8192, 196608 in all
- norm_gain: float32 [2, 4096], P(None, 'dp'), may hold values from 0.1 to 1.9
- gate_proj: bfloat16 [2, 4096, 4096], P(None, 'dp', 'tp'), may hold values from -0.09375 to 0.09375
- input_proj: bfloat16 [2, 4096, 4096], P(None, 'dp', 'tp'), may hold values from -0.09375 to 0.09375
- coupling_proj: bfloat16 [2, 4096, 2, 2048], P(None, 'dp', None, 'tp'), may hold values from -0.09375 to 0.09375
- step_proj: bfloat16 [2, 4096, 64], P(None, 'dp'), may hold values from -0.09375 to 0.09375
- input_taps: float32 [2, 5, 4096], P(None, None, 'tp'), may hold values from -2.5 to 2.5
- coupling_taps: float32 [2, 5, 2, 2048], P(None, None, None, 'tp'), may hold values from -2.5 to 2.5
- step_bias: float32 [2, 64], replicated, may hold values from -5 to -1
- decay_log: float32 [2, 64], replicated, may hold values from -1 to 2.5
- skip_gain: float32 [2, 64], replicated, may hold values from 0.1 to 3
- span_bias: float32 [2, 8, 64], replicated, may hold values from -2 to 2
- mix_gain: float32 [2, 4096], P(None, 'tp'), may hold values from 0.1 to 1.9
- out_proj: bfloat16 [2, 4096, 4096], P(None, 'tp', 'dp'), may hold values from -0.09375 to 0.09375
- recurrent: float32 [2, 96, 64, 64, 128], P(None, 'dp', 'tp'), may hold values from -1.2 to 1.2
- input_history: bfloat16 [2, 96, 4, 4096], P(None, 'dp', None, 'tp'), may hold values from -6 to 6
- coupling_history: bfloat16 [2, 96, 4, 2, 2048], P(None, 'dp', None, None, 'tp'), may hold values from -6 to 6
Outputs:
- out_hidden: bfloat16 [96, 4096], P(None, 'dp')
- new_recurrent: float32 [2, 96, 64, 64, 128], P(None, 'dp', 'tp')
- next_inputs: bfloat16 [2, 96, 4, 4096], P(None, 'dp', None, 'tp')
- next_couplings: bfloat16 [2, 96, 4, 2, 2048], P(None, 'dp', None, None, 'tp')
Inputs may be any that keep to these rules, and one draw needn't show every extreme that they name: `lengths`: every sequence's length; the longest is exactly 8192, and they sum to 2048 times the number of sequences.
All inputs are finite; a program needn't handle non-finite values. No bound on the sum of `lengths` on one device may be relied on, other than what follows from the above.
Results may differ from a plain program's by a relative error of at most 0.02.
Values may be sent and summed in bfloat16 or wider, within the bound.
A program may use at most 128 MiB of HBM per device.

v0:
```python
import jax
import jax.numpy as jnp
from jax import lax
from jax.sharding import PartitionSpec as P

D = 4096
HEAD_DIM = 64
STATE = 128
LAYERS = 2
SPAN_LEN = 1024
INNER = 4096
SPANS = 8


EPS = 1e-06


def head_slice(param_table, take_count):
    return lax.dynamic_slice_in_dim(
        param_table, lax.axis_index("tp") * take_count, take_count, param_table.ndim - 1
    )


def norm_rows(rows, gain):
    values = rows.astype(jnp.float32)
    squares = lax.psum(jnp.sum(values * values, axis=1), "dp")
    return (values * lax.rsqrt(squares / D + EPS)[:, None] * gain[None, :]).astype(jnp.bfloat16)


def mixer_layer(normed, lengths, weights, histories):
    (
        gate_proj,
        input_proj,
        coupling_proj,
        step_proj,
        input_taps,
        coupling_taps,
        step_bias,
        decay_log,
        skip_gain,
        span_bias,
        mix_gain,
        out_proj,
    ) = weights
    recurrent, input_history, coupling_history = histories
    local_heads = recurrent.shape[1]
    local_groups = coupling_proj.shape[2] // STATE
    per_group = local_heads // local_groups
    gate_part = jnp.dot(normed, gate_proj, preferred_element_type=jnp.float32)
    input_part = jnp.dot(normed, input_proj, preferred_element_type=jnp.float32)
    coupling_part = jnp.dot(
        normed,
        coupling_proj.reshape(coupling_proj.shape[0], -1),
        preferred_element_type=jnp.float32,
    )
    step_part = jnp.dot(
        normed, head_slice(step_proj, local_heads), preferred_element_type=jnp.float32
    )
    gate_sum, input_sum, coupling_sum, step_sum = (
        lax.psum_scatter(
            gate_part.astype(jnp.bfloat16), "dp", scatter_dimension=0, tiled=True
        ).astype(jnp.float32),
        lax.psum_scatter(
            input_part.astype(jnp.bfloat16), "dp", scatter_dimension=0, tiled=True
        ).astype(jnp.float32),
        lax.psum_scatter(
            coupling_part.astype(jnp.bfloat16), "dp", scatter_dimension=0, tiled=True
        ).astype(jnp.float32),
        lax.psum_scatter(
            step_part.astype(jnp.bfloat16), "dp", scatter_dimension=0, tiled=True
        ).astype(jnp.float32),
    )
    gate_in, input_in, coupling_flat, step_in = lax.optimization_barrier(
        (
            gate_sum.astype(jnp.bfloat16),
            input_sum.astype(jnp.bfloat16),
            coupling_sum.astype(jnp.bfloat16),
            step_sum.astype(jnp.bfloat16),
        )
    )
    row_count = input_in.shape[0]
    coupling_in = coupling_flat.reshape(row_count, 2, -1)
    input_window = jnp.concatenate([input_history, input_in[:, None, :]], axis=1)
    coupling_window = jnp.concatenate([coupling_history, coupling_in[:, None]], axis=1)
    input_act = jax.nn.silu(jnp.sum(input_window.astype(jnp.float32) * input_taps[None], axis=1))
    coupling_act = jax.nn.silu(
        jnp.sum(coupling_window.astype(jnp.float32) * coupling_taps[None], axis=1)
    )
    span_index = (lengths - 1) // SPAN_LEN
    onehot = (span_index[:, None] == jnp.arange(SPANS, dtype=jnp.int32)[None, :]).astype(
        jnp.float32
    )
    span_term = jnp.sum(onehot[:, :, None] * head_slice(span_bias, local_heads)[None], axis=1)
    step_size = jax.nn.softplus(
        step_in.astype(jnp.float32) + head_slice(step_bias, local_heads)[None] + span_term
    )
    decay_rate = jnp.exp(-step_size * jnp.exp(head_slice(decay_log, local_heads))[None])
    input_heads = input_act.reshape(row_count, local_groups, per_group, HEAD_DIM)
    write_vec = coupling_act[:, 0].reshape(row_count, local_groups, STATE)
    read_vec = coupling_act[:, 1].reshape(row_count, local_groups, STATE)
    drive = step_size.reshape(row_count, local_groups, per_group)[..., None] * input_heads
    prior_state = recurrent.reshape(row_count, local_groups, per_group, HEAD_DIM, STATE)
    fresh_state = (
        decay_rate.reshape(row_count, local_groups, per_group)[..., None, None] * prior_state
        + drive[..., None] * write_vec[:, :, None, None, :]
    )
    readout = jnp.einsum("sgrpn,sgn->sgrp", fresh_state, read_vec, precision=lax.Precision.HIGHEST)
    readout = (
        readout
        + head_slice(skip_gain, local_heads).reshape(1, local_groups, per_group, 1) * input_heads
    )
    gated_out = readout.reshape(row_count, -1) * jax.nn.silu(gate_in.astype(jnp.float32))
    squares = lax.psum(jnp.sum(gated_out * gated_out, axis=1), "tp")
    mixed = (gated_out * lax.rsqrt(squares / INNER + EPS)[:, None] * mix_gain[None]).astype(
        jnp.bfloat16
    )
    out_terms = jnp.dot(
        lax.all_gather(mixed, "dp", axis=0, tiled=True),
        out_proj,
        preferred_element_type=jnp.float32,
    )
    new_state = fresh_state.reshape(row_count, local_heads, HEAD_DIM, STATE)
    return (out_terms, new_state, input_window[:, 1:], coupling_window[:, 1:])


def on_device(
    hidden,
    lengths,
    norm_gain,
    gate_proj,
    input_proj,
    coupling_proj,
    step_proj,
    input_taps,
    coupling_taps,
    step_bias,
    decay_log,
    skip_gain,
    span_bias,
    mix_gain,
    out_proj,
    recurrent,
    input_history,
    coupling_history,
):
    share_rows = hidden.shape[0] // lax.axis_size("tp")
    first_row = lax.axis_index("tp") * share_rows
    stream = hidden
    normed = norm_rows(hidden, norm_gain[0])
    states, inputs_next, couplings_next = ([], [], [])
    for layer_index in range(LAYERS):
        weights = (
            gate_proj[layer_index],
            input_proj[layer_index],
            coupling_proj[layer_index],
            step_proj[layer_index],
            input_taps[layer_index],
            coupling_taps[layer_index],
            step_bias[layer_index],
            decay_log[layer_index],
            skip_gain[layer_index],
            span_bias[layer_index],
            mix_gain[layer_index],
            out_proj[layer_index],
        )
        histories = (
            recurrent[layer_index],
            input_history[layer_index],
            coupling_history[layer_index],
        )
        out_terms, new_state, input_recent, coupling_recent = mixer_layer(
            normed, lengths, weights, histories
        )
        states.append(new_state)
        inputs_next.append(input_recent)
        couplings_next.append(coupling_recent)
        summed = lax.psum_scatter(
            out_terms.astype(jnp.bfloat16), "tp", scatter_dimension=0, tiled=True
        ).astype(jnp.float32)
        if layer_index == 0:
            stream = lax.dynamic_slice_in_dim(stream, first_row, share_rows, 0)
        stream = (stream.astype(jnp.float32) + summed).astype(jnp.bfloat16)
        if layer_index + 1 < LAYERS:
            normed = lax.all_gather(
                norm_rows(stream, norm_gain[layer_index + 1]), "tp", axis=0, tiled=True
            )
    stream = lax.all_gather(stream, "tp", axis=0, tiled=True)
    return (stream, jnp.stack(states), jnp.stack(inputs_next), jnp.stack(couplings_next))


def solution(mesh):
    placed = (
        P(None, "dp"),
        P("dp"),
        P(None, "dp"),
        P(None, "dp", "tp"),
        P(None, "dp", "tp"),
        P(None, "dp", None, "tp"),
        P(None, "dp", None),
        P(None, None, "tp"),
        P(None, None, None, "tp"),
        P(),
        P(),
        P(),
        P(),
        P(None, "tp"),
        P(None, "tp", "dp"),
        P(None, "dp", "tp", None, None),
        P(None, "dp", None, "tp"),
        P(None, "dp", None, None, "tp"),
    )
    return jax.shard_map(
        on_device,
        mesh=mesh,
        in_specs=placed,
        out_specs=(
            P(None, "dp"),
            P(None, "dp", "tp", None, None),
            P(None, "dp", None, "tp"),
            P(None, "dp", None, None, "tp"),
        ),
        check_vma=False,
    )
```

profile of v0, /device:TPU:0, one launch (start us, length us, event | category | flops | bytes accessed | tf_op | source)
XLA Modules:
  0.0 396.1 jit_solution(17236018546369188771)
XLA Ops:
  7.3 1.4 fusion.28
  8.8 8.4 %psum.28 = f32[96]{0:T(128)S(1)} all-reduce(f32[96]{0:T(128)S(1)} %fusion.28), channel_id=1, replica_groups=mesh['tp'=8,'dp'=4] {'dp'}, use_global_device_ids=true, to_apply=%region_1.0 | all-reduce | flops 96 | bytes 768 | tf_op jit(solution)/shard_map/psum | solution.py:26
  17.2 0.8 fusion.75
  17.9 2.3 convolution_convert_fusion.6
  20.4 2.3 convolution_convert_fusion.7
  22.8 2.7 fusion.72
  25.4 0.2 copy.86
  25.7 1.0 convolution_convert_fusion.5
  26.8 0.6 dynamic-slice.20
  28.0 0.1 slice_bitcast_fusion
  28.2 0.2 convolution_convert_fusion.9
  28.4 5.7 %all-reduce = bf16[96,8]{0,1:T(8,128)(2,1)S(1)} all-reduce(bf16[96,8]{0,1:T(8,128)(2,1)S(1)} %convolution_convert_fusion.9), channel_id=5, replica_groups=mesh['tp'=8,'dp'=4] {'dp'}, use_global_device_ids=true, to_apply=%region_5.0.clone | all-reduce | flops 768 | bytes 3072
  34.1 0.2 copy.87
  34.4 6.6 %slice.128 = f32[1,24,8,64,128]{4,3,2,1,0:T(8,128)} slice(f32[2,24,8,64,128]{4,3,2,1,0:T(8,128)} %param.33), slice={[0:1], [0:24], [0:8], [0:64], [0:128]} | slice | bytes 12582912 | tf_op jit(solution)/shard_map/slice | solution.py:167
  41.6 0.6 dynamic-slice.10
  43.2 19.9 %reduce-scatter.13.cloned.1.call-done = bf16[24,512]{1,0:T(8,128)(2,1)} async-done(((bf16[96,512]{1,0:T(8,128)(2,1)}), bf16[24,512]{1,0:T(8,128)(2,1)}) %reduce-scatter.13.cloned.1.call-update) | async-done | bytes 24592 | tf_op jit(solution)/shard_map/reduce_scatter | solution.py:60
  63.1 22.7 %reduce-scatter.17.cloned.1.call-done = bf16[24,512]{1,0:T(8,128)(2,1)} async-done(((bf16[96,512]{1,0:T(8,128)(2,1)}), bf16[24,512]{1,0:T(8,128)(2,1)}) %reduce-scatter.17.cloned.1.call-update) | async-done | bytes 24592 | tf_op jit(solution)/shard_map/reduce_scatter | solution.py:66
  85.9 0.8 copy.64
  86.9 0.8 broadcast_in_dim_reshape.4
  87.6 0.1 fusion.36
  87.8 0.2 multiply_reduce_fusion.1
  88.0 0.2 multiply_reduce_fusion.3
  88.5 16.9 %fusion.6 = f32[24,2,1,4,64]{4,2,3,1,0:T(1,128)S(1)} fusion(f32[24,2,4,64,128]{4,3,2,1,0:T(8,128)} %bitcast.124, f32[24,2,128]{2,1,0:T(2,128)S(1)} %bitcast.138, f32[24,2,4,64]{3,2,1,0:T(4,128)S(1)} %broadcast_multiply_fusion.1, f32[24,2,4]{2,1,0:T(2,128)S(1)} %copy.62, f32[24,2,256]{2,1,0:T(2,128)S(1)} %divide_multiply_fusion.3), kind=kOutput, calls=%fused_computation.7 | convolution fusion | flops 23592960 | bytes 6512640 | tf_op jit(solution)/shard_map/sgrpn,sgn->sgrp/dot_general | solution.py:107
  105.6 0.1 multiply_reduce_fusion.5
  105.8 21.3 %psum.29 = f32[24]{0:T(128)S(1)} all-reduce(f32[24]{0:T(128)S(1)} %multiply_reduce_fusion.5), channel_id=1, replica_groups=mesh['tp'=8,'dp'=4] {'tp'}, use_global_device_ids=true, to_apply=%region_10.11 | all-reduce | flops 24 | bytes 192 | tf_op jit(solution)/shard_map/psum | solution.py:113
  127.2 5.3 %all_gather.12 = bf16[96,512]{1,0:T(8,128)(2,1)S(1)} all-gather(bf16[24,512]{1,0:T(8,128)(2,1)S(1)} %multiply_convert_fusion.1), channel_id=1, replica_groups=mesh['tp'=8,'dp'=4] {'dp'}, dimensions={0}, use_global_device_ids=true | all-gather | bytes 122880 | tf_op jit(solution)/shard_map/all_gather | solution.py:118
  132.5 1.5 convolution_convert_fusion.1
  134.1 20.6 %fusion = bf16[16,1024]{1,0:T(8,128)(2,1)S(1)} fusion(bf16[96,1024]{1,0:T(8,128)(2,1)S(1)} %convolution_convert_fusion.1), kind=kCustom, calls=%all-reduce-scatter | all-reduce-scatter fusion | flops 131073 | bytes 229888
  154.7 2.1 collective-permute-start
  156.8 1.3 collective-permute-start.1
  158.2 0.1 fusion.37
  158.4 1.3 collective-permute-done.1
  159.7 0.3 concatenate.16
  160.0 0.1 fusion.39
  160.1 6.0 %psum.30 = f32[12]{0:T(128)S(1)} all-reduce(f32[12]{0:T(128)S(1)} %get-tuple-element.24), channel_id=1, replica_groups=mesh['tp'=8,'dp'=4] {'dp'}, use_global_device_ids=true, to_apply=%region_13.14 | all-reduce | flops 12 | bytes 96 | tf_op jit(solution)/shard_map/psum | solution.py:26
  166.2 31.2 %all-gather = bf16[8,12,1024]{2,1,0:T(8,128)(2,1)S(1)} all-gather(bf16[1,12,1024]{2,1,0:T(8,128)(2,1)S(1)} %fusion.52), channel_id=1, replica_groups=mesh['tp'=8,'dp'=4] {'tp'}, dimensions={0}, use_global_device_ids=true | all-gather | bytes 221184 | tf_op jit(solution)/shard_map/all_gather | solution.py:184
  197.4 1.0 convolution_convert_fusion.2
  198.4 2.2 convolution_convert_fusion.4
  200.7 2.2 convolution_convert_fusion.3
  202.9 0.2 convolution_convert_fusion.8
  203.0 5.8 %all-reduce.2 = bf16[96,8]{0,1:T(8,128)(2,1)S(1)} all-reduce(bf16[96,8]{0,1:T(8,128)(2,1)S(1)} %convolution_convert_fusion.8), channel_id=10, replica_groups=mesh['tp'=8,'dp'=4] {'dp'}, use_global_device_ids=true, to_apply=%region_17.18.clone | all-reduce | flops 768 | bytes 3072
  208.9 7.2 %reduce-scatter.23.cloned.1.call-done = bf16[24,512]{1,0:T(8,128)(2,1)} async-done(((bf16[96,512]{1,0:T(8,128)(2,1)}), bf16[24,512]{1,0:T(8,128)(2,1)}) %reduce-scatter.23.cloned.1.call-update) | async-done | bytes 24592 | tf_op jit(solution)/shard_map/reduce_scatter | solution.py:66
  216.1 22.5 %reduce-scatter.19.cloned.1.call-done = bf16[24,512]{1,0:T(8,128)(2,1)} async-done(((bf16[96,512]{1,0:T(8,128)(2,1)}), bf16[24,512]{1,0:T(8,128)(2,1)}) %reduce-scatter.19.cloned.1.call-update) | async-done | bytes 24592 | tf_op jit(solution)/shard_map/reduce_scatter | solution.py:60
  238.6 22.5 %reduce-scatter.21.cloned.1.call-done = bf16[24,512]{1,0:T(8,128)(2,1)} async-done(((bf16[96,512]{1,0:T(8,128)(2,1)}), bf16[24,512]{1,0:T(8,128)(2,1)}) %reduce-scatter.21.cloned.1.call-update) | async-done | bytes 24592 | tf_op jit(solution)/shard_map/reduce_scatter | solution.py:63
  261.1 0.8 copy.69
  261.8 0.1 fusion.34
  262.0 0.2 multiply_reduce_fusion
  262.8 0.8 broadcast_in_dim_reshape.5
  263.6 0.2 multiply_reduce_fusion.2
  264.1 10.8 %multiply_add_fusion.1 = (f32[1,24,8,64,128]{4,3,2,1,0:T(8,128)}, f32[1,24,8,64,128]{4,3,2,1,0:T(8,128)}, f32[1,24,8,64,128]{4,3,2,1,0:T(8,128)S(1)}) fusion(f32[24,8,128]{2,1,0:T(8,128)S(1)} %bitcast.130, f32[24,8,64]{2,1,0:T(8,128)S(1)} %multiply_multiply_fusion.1, f32[24,8]{1,0:T(8,128)S(1)} %copy.72, f32[2,24,8,64,128]{4,3,2,1,0:T(8,128)} %param.33, ...), kind=kLoop, calls=%fused_computation.2 | loop fusion | flops 9437184 | bytes 31753728 | tf_op jit(solution)/shard_map/add | solution.py:104
  275.0 15.8 %fusion.2 = f32[24,2,1,4,64]{4,2,3,1,0:T(1,128)S(1)} fusion(f32[24,2,4,64,128]{4,3,2,1,0:T(8,128)S(1)} %bitcast.125, f32[24,2,128]{2,1,0:T(2,128)S(1)} %bitcast.141, f32[24,2,4,64]{3,2,1,0:T(4,128)S(1)} %broadcast_multiply_fusion, f32[24,2,4]{2,1,0:T(2,128)S(1)} %copy.67, f32[24,2,256]{2,1,0:T(2,128)S(1)} %divide_multiply_fusion.2), kind=kOutput, calls=%fused_computation.3 | convolution fusion | flops 23592960 | bytes 6512640 | tf_op jit(solution)/shard_map/sgrpn,sgn->sgrp/dot_general | solution.py:107
  291.0 0.1 multiply_reduce_fusion.4
  291.2 21.4 %psum.31 = f32[24]{0:T(128)S(1)} all-reduce(f32[24]{0:T(128)S(1)} %multiply_reduce_fusion.4), channel_id=1, replica_groups=mesh['tp'=8,'dp'=4] {'tp'}, use_global_device_ids=true, to_apply=%region_22.23 | all-reduce | flops 24 | bytes 192 | tf_op jit(solution)/shard_map/psum | solution.py:113
  312.7 5.3 %all_gather.14 = bf16[96,512]{1,0:T(8,128)(2,1)S(1)} all-gather(bf16[24,512]{1,0:T(8,128)(2,1)S(1)} %multiply_convert_fusion), channel_id=1, replica_groups=mesh['tp'=8,'dp'=4] {'dp'}, dimensions={0}, use_global_device_ids=true | all-gather | bytes 122880 | tf_op jit(solution)/shard_map/all_gather | solution.py:118
  318.0 1.5 convolution_convert_fusion
  319.5 20.6 %fusion.1 = bf16[16,1024]{1,0:T(8,128)(2,1)S(1)} fusion(bf16[96,1024]{1,0:T(8,128)(2,1)S(1)} %convolution_convert_fusion), kind=kCustom, calls=%all-reduce-scatter.1 | all-reduce-scatter fusion | flops 131073 | bytes 229888
  340.1 2.1 collective-permute-start.2
  342.3 1.3 collective-permute-start.3
  343.6 0.8 pad_maximum_fusion.3
  344.4 12.1 %pad_maximum_fusion = f32[2,24,8,64,128]{4,3,2,1,0:T(8,128)} fusion(f32[1,24,8,64,128]{4,3,2,1,0:T(8,128)} %get-tuple-element.29, f32[1,24,8,64,128]{4,3,2,1,0:T(8,128)} %get-tuple-element.28), kind=kLoop, calls=%fused_computation | loop fusion | flops 3145728 | bytes 25165824 | tf_op jit(solution)/shard_map/stack | solution.py:188
  356.5 1.0 pad_maximum_fusion.4
  357.5 0.3 concatenate.17
  357.8 30.8 %all-gather.1 = bf16[8,12,1024]{2,1,0:T(8,128)(2,1)S(1)} all-gather(bf16[1,12,1024]{2,1,0:T(8,128)(2,1)S(1)} %fusion.51), channel_id=1, replica_groups=mesh['tp'=8,'dp'=4] {'tp'}, dimensions={0}, use_global_device_ids=true | all-gather | bytes 221184 | tf_op jit(solution)/shard_map/all_gather | solution.py:187
  388.6 0.7 reshape.125
  (110 shorter events, 4.2 us)
Async XLA Ops:
  7.2 19.6 %copy-start.13 = (u32[32]{0:T(128)S(1)}, u32[32]{0:T(128)}, u32[]{:S(2)}) copy-start(u32[32]{0:T(128)} %constant.77) | copy-start | bytes 388
  7.2 18.5 %copy-start = (bf16[96,1024]{1,0:T(8,128)(2,1)S(1)}, bf16[96,1024]{1,0:T(8,128)(2,1)}, u32[]{:S(2)}) copy-start(bf16[96,1024]{1,0:T(8,128)(2,1)} %param.18) | copy-start | bytes 589828
  7.2 20.2 %copy-start.14 = (s32[24]{0:T(128)S(1)}, s32[24]{0:T(128)}, u32[]{:S(2)}) copy-start(s32[24]{0:T(128)} %param.19) | copy-start | bytes 292
  7.2 20.2 %copy-start.10 = (f32[2,64]{1,0:T(2,128)S(1)}, f32[2,64]{1,0:T(2,128)}, u32[]{:S(2)}) copy-start(f32[2,64]{1,0:T(2,128)} %param.27) | copy-start | bytes 1540
  7.2 20.2 %copy-start.11 = (f32[2,64]{1,0:T(2,128)S(1)}, f32[2,64]{1,0:T(2,128)}, u32[]{:S(2)}) copy-start(f32[2,64]{1,0:T(2,128)} %param.28) | copy-start | bytes 1540
  7.2 20.2 %copy-start.12 = (f32[2,64]{1,0:T(2,128)S(1)}, f32[2,64]{1,0:T(2,128)}, u32[]{:S(2)}) copy-start(f32[2,64]{1,0:T(2,128)} %param.29) | copy-start | bytes 1540
  7.2 20.6 %copy-start.8 = (f32[2,8,64]{2,1,0:T(8,128)S(1)}, f32[2,8,64]{2,1,0:T(8,128)}, u32[]{:S(2)}) copy-start(f32[2,8,64]{2,1,0:T(8,128)} %param.30) | copy-start | bytes 12292
  7.2 20.6 %copy-start.6 = (f32[2,5,512]{2,0,1:T(2,128)S(1)}, f32[2,5,512]{2,0,1:T(2,128)}, u32[]{:S(2)}) copy-start(f32[2,5,512]{2,0,1:T(2,128)} %param.25) | copy-start | bytes 61444
  7.3 20.6 %copy-start.7 = (f32[2,5,2,256]{3,2,1,0:T(2,128)S(1)}, f32[2,5,2,256]{3,2,1,0:T(2,128)}, u32[]{:S(2)}) copy-start(f32[2,5,2,256]{3,2,1,0:T(2,128)} %param.26) | copy-start | bytes 61444
  7.3 20.6 %copy-start.2 = (bf16[2,24,4,512]{3,2,1,0:T(4,128)(2,1)S(1)}, bf16[2,24,4,512]{3,2,1,0:T(4,128)(2,1)}, u32[]{:S(2)}) copy-start(bf16[2,24,4,512]{3,2,1,0:T(4,128)(2,1)} %param.34) | copy-start | bytes 589828
  7.3 20.7 %copy-start.3 = (bf16[2,24,4,2,256]{4,3,2,1,0:T(2,128)(2,1)S(1)}, bf16[2,24,4,2,256]{4,3,2,1,0:T(2,128)(2,1)}, u32[]{:S(2)}) copy-start(bf16[2,24,4,2,256]{4,3,2,1,0:T(2,128)(2,1)} %param.35) | copy-start | bytes 589828
  7.3 20.8 %copy-start.1 = (bf16[2,1024,64]{1,2,0:T(8,128)(2,1)S(1)}, bf16[2,1024,64]{1,2,0:T(8,128)(2,1)}, u32[]{:S(2)}) copy-start(bf16[2,1024,64]{1,2,0:T(8,128)(2,1)} %param.24) | copy-start | bytes 786436
  7.3 35.9 %reduce-scatter.15.cloned.1.call-start = ((), (), s32[]{:S(2)}) async-start(), calls=%async_computation.7 | async-start | bytes 122880 | tf_op jit(solution)/shard_map/reduce_scatter | solution.py:63
  20.3 42.8 %reduce-scatter.13.cloned.1.call-start = ((), (), s32[]{:S(2)}) async-start(), calls=%async_computation.6 | async-start | bytes 122880 | tf_op jit(solution)/shard_map/reduce_scatter | solution.py:60
  22.7 63.0 %reduce-scatter.17.cloned.1.call-start = ((), (), s32[]{:S(2)}) async-start(), calls=%async_computation.8 | async-start | bytes 122880 | tf_op jit(solution)/shard_map/reduce_scatter | solution.py:66
  26.7 189.3 %reduce-scatter.23.cloned.1.call-start = ((), (), s32[]{:S(2)}) async-start(), calls=%async_computation.11 | async-start | bytes 122880 | tf_op jit(solution)/shard_map/reduce_scatter | solution.py:66
  34.4 7.2 %copy-start.15 = (u32[32]{0:T(128)S(1)}, u32[32]{0:T(128)}, u32[]{:S(2)}) copy-start(u32[32]{0:T(128)} %constant.73) | copy-start | bytes 388
  34.4 8.8 %copy-start.9 = (f32[2,512]{1,0:T(2,128)S(1)}, f32[2,512]{1,0:T(2,128)}, u32[]{:S(2)}) copy-start(f32[2,512]{1,0:T(2,128)} %param.31) | copy-start | bytes 12292
  63.1 42.5 %copy-start.4 = (bf16[24,512]{1,0:T(8,128)(2,1)S(1)}, bf16[24,512]{1,0:T(8,128)(2,1)}, u32[]{:S(2)}) copy-start(bf16[24,512]{1,0:T(8,128)(2,1)} %reduce-scatter.13.cloned.1.call-done) | copy-start | bytes 73732
  154.7 5.0 %collective-permute-start = (bf16[16,1024]{1,0:T(8,128)(2,1)S(1)}, bf16[16,1024]{1,0:T(8,128)(2,1)S(1)}, u32[]{:S(2)}, u32[]{:S(2)}) collective-permute-start(bf16[16,1024]{1,0:T(8,128)(2,1)S(1)} %fusion), channel_id=1, source_target_pairs={{0,4},{4,8},{8,12},{12,16},{16,20},{20,24},{24,28},{1,5},{5,9},{9,... | collective-permute-start | bytes 98312
  156.8 2.9 collective-permute-start.1
  198.4 40.2 %reduce-scatter.19.cloned.1.call-start = ((), (), s32[]{:S(2)}) async-start(), calls=%async_computation.9 | async-start | bytes 122880 | tf_op jit(solution)/shard_map/reduce_scatter | solution.py:60
  200.6 60.4 %reduce-scatter.21.cloned.1.call-start = ((), (), s32[]{:S(2)}) async-start(), calls=%async_computation.10 | async-start | bytes 122880 | tf_op jit(solution)/shard_map/reduce_scatter | solution.py:63
  274.9 16.0 %copy-start.5 = (bf16[24,512]{1,0:T(8,128)(2,1)S(1)}, bf16[24,512]{1,0:T(8,128)(2,1)}, u32[]{:S(2)}) copy-start(bf16[24,512]{1,0:T(8,128)(2,1)} %reduce-scatter.19.cloned.1.call-done) | copy-start | bytes 73732
  340.1 17.3 %collective-permute-start.2 = (bf16[16,1024]{1,0:T(8,128)(2,1)S(1)}, bf16[16,1024]{1,0:T(8,128)(2,1)S(1)}, u32[]{:S(2)}, u32[]{:S(2)}) collective-permute-start(bf16[16,1024]{1,0:T(8,128)(2,1)S(1)} %fusion.1), channel_id=1, source_target_pairs={{0,4},{4,8},{8,12},{12,16},{16,20},{20,24},{24,28},{1,5},{5,9},{9,... | collective-permute-start | bytes 98312
  342.3 15.2 %collective-permute-start.3 = (bf16[12,1024]{1,0:T(8,128)(2,1)S(1)}, bf16[12,1024]{1,0:T(8,128)(2,1)S(1)}, u32[]{:S(2)}, u32[]{:S(2)}) collective-permute-start(bf16[12,1024]{1,0:T(8,128)(2,1)S(1)} %slice.173), channel_id=1, source_target_pairs={{0,8},{4,12},{8,16},{12,20},{16,24},{20,28},{1,9},{5,13},{9,17},{1... | collective-permute-start | bytes 73736
Sparse Core Ops, SparseCore 0:
  20.4 19.9 reduce-scatter.14
  43.4 19.6 reduce-scatter.12
  66.1 19.6 reduce-scatter.16
  198.5 17.5 reduce-scatter.22
  218.9 19.6 reduce-scatter.18
  241.4 19.6 reduce-scatter.20
where the time goes:
time: 397 us; the launch traced here: 396 us
  blocking collectives  182 us (46%)
  waiting for transfers between devices  96.1 us (24%)
  matrix products  47.1 us (12%)
  other arithmetic  29.2 us (7%)
  local copies, waits for them, and re-layouts  18.7 us (5%)
  between operations  15.9 us (4%)
  starting transfers between devices  7.09 us (2%)
    unnamed x4, blocking collectives  52.6 us
    psum x2, blocking collectives, mixer_layer(): squares = lax.psum(jnp.sum(gated_out * gated_out, axis=1), 'tp')  42.7 us
    reduce_scatter x2, waiting for transfers between devices, mixer_layer(): lax.psum_scatter(gate_part.astype(jnp.bfloat16), 'dp', scatter_dimension=...  42.3 us
    dot_general x2, matrix products, mixer_layer(): jnp.einsum('sgrpn,sgn->sgrp', fresh_state, read_vec, precision=lax.Precis...  32.7 us
    all_gather x1, blocking collectives, on_device(): lax.all_gather(norm_rows(stream, norm_gain[layer_index + 1]), 'tp', axis=...  31.2 us
    all_gather x1, blocking collectives, on_device(): stream = lax.all_gather(stream, 'tp', axis=0, tiled=True)  30.8 us
    reduce_scatter x2, waiting for transfers between devices, mixer_layer(): lax.psum_scatter(coupling_part.astype(jnp.bfloat16), 'dp', scatter_dimens...  29.8 us
    reduce_scatter x2, waiting for transfers between devices, mixer_layer(): lax.psum_scatter(input_part.astype(jnp.bfloat16), 'dp', scatter_dimension...  22.5 us
  transfers between devices with their start and end apart: 10, of which 6 were waited for; matrix products, arithmetic and copies ran while one was open for 9% of the time, Pallas kernels for 0%

commit v1 on v0

v1 whole, which is shorter than its diff:
```python
import functools

import jax
import jax.numpy as jnp
from jax import lax
from jax.experimental import pallas as pl
from jax.experimental.pallas import tpu as pltpu
from jax.sharding import PartitionSpec as P

HEAD_DIM = 64
STATE = 128
LAYERS = 2
SPAN_LEN = 1024
SPANS = 8
LANES = 128
ROWS = 8
EPS = 1e-06
VMEM_LIMIT = 40 * 1024 * 1024
MESH = pl.DeviceIdType.MESH
F32 = jnp.float32
BF16 = jnp.bfloat16


def head_slice(param_table, take_count):
    return lax.dynamic_slice_in_dim(
        param_table, lax.axis_index("tp") * take_count, take_count, param_table.ndim - 1
    )


def greet(axes):
    barrier = pltpu.get_barrier_semaphore()
    total = 0
    for axis, count in axes:
        me = lax.axis_index(axis)
        for k in range(1, count):
            pl.semaphore_signal(
                barrier, inc=1, device_id={axis: lax.rem(me + k, count)}, device_id_type=MESH
            )
            total += 1
    pl.semaphore_wait(barrier, total)


def remote(src, dst, send_sem, recv_sem, axis, peer):
    return pltpu.make_async_remote_copy(
        src_ref=src,
        dst_ref=dst,
        send_sem=send_sem,
        recv_sem=recv_sem,
        device_id={axis: peer},
        device_id_type=MESH,
    )


def split_sum(squares, width=LANES):
    high = squares.astype(BF16).astype(F32)
    low = squares - high
    lane = lax.broadcasted_iota(jnp.int32, (squares.shape[0], width), 1)
    return jnp.where(lane == 0, high, jnp.where(lane == 1, low, 0.0))


def project_kernel(
    n_dp, rows, features, x_ref, gain_ref, gate_ref, input_ref, coup_ref, step_ref,
    out_ref, send_buf, recv_buf, send_sem, recv_sem,
):
    me = lax.axis_index("dp")
    greet((("dp", n_dp),))
    values = x_ref[...].astype(F32)
    squares = jnp.sum(values * values, axis=1, keepdims=True)
    scaled = (values * gain_ref[...]).astype(BF16)

    def put(first, block):
        for d in range(n_dp):
            send_buf[d, :, first:first + block.shape[1]] = block[d * rows:(d + 1) * rows].astype(BF16)

    first = 0
    for ref in (gate_ref, input_ref, coup_ref):
        weight = ref[0] if len(ref.shape) == 3 else ref[...]
        put(first, jnp.dot(scaled, weight, preferred_element_type=F32))
        first += weight.shape[1]
    steps = lax.dot_general(
        scaled, step_ref[0], (((1,), (1,)), ((), ())), preferred_element_type=F32
    )
    spare = -steps.shape[1] % LANES
    if spare:
        steps = jnp.concatenate([steps, jnp.zeros((steps.shape[0], spare), F32)], axis=1)
    put(first, steps)
    first += steps.shape[1]
    put(first, split_sum(squares))

    copies = []
    for k in range(1, n_dp):
        peer = lax.rem(me + k, n_dp)
        copy = remote(
            send_buf.at[peer], recv_buf.at[k - 1], send_sem.at[k - 1], recv_sem.at[k - 1], "dp", peer
        )
        copy.start()
        copies.append(copy)
    total = send_buf[me].astype(F32)
    for k in range(1, n_dp):
        copies[k - 1].wait_recv()
        total = total + recv_buf[k - 1].astype(F32)
    squares = total[:, first:first + 1] + total[:, first + 1:first + 2]
    out_ref[...] = total[:, :first] * lax.rsqrt(squares / features + EPS)
    for copy in copies:
        copy.wait_send()


def state_kernel(
    heads, per_group, drive_ref, decay_ref, write_ref, read_ref, skip_ref, gate_ref, gain_ref,
    prior_ref, *rest,
):
    fresh_ref, gated_ref = rest[-2], rest[-1]
    drive_t = jnp.transpose(drive_ref[...])
    lane = lax.broadcasted_iota(jnp.int32, (HEAD_DIM, LANES), 1)
    sums = [jnp.zeros((HEAD_DIM, LANES), F32) for _ in range(heads)]
    for j in range(ROWS):
        for h in range(heads):
            g = h // per_group
            write = write_ref[j:j + 1, g * STATE:(g + 1) * STATE]
            read = read_ref[j:j + 1, g * STATE:(g + 1) * STATE]
            column = drive_t[h * HEAD_DIM:(h + 1) * HEAD_DIM, j:j + 1]
            fresh = decay_ref[j, h:h + 1, :] * prior_ref[0, j, h] + column * write
            fresh_ref[0, j, h] = fresh
            total = jnp.sum(fresh * read, axis=1, keepdims=True)
            sums[h] = jnp.where(lane == j, total, sums[h])
    readout = jnp.transpose(jnp.concatenate(sums, axis=0))[:ROWS]
    gated = (readout + skip_ref[...]) * gate_ref[...]
    squares = jnp.sum(gated * gated, axis=1, keepdims=True)
    inner = gated.shape[1]
    gated_ref[:, :inner] = gated * gain_ref[...]
    gated_ref[:, inner:] = split_sum(squares)


def output_kernel(
    n_dp, n_tp, rows, share, inner, gated_ref, weight_ref, stream_ref, out_ref,
    mine_buf, gather_buf, part_buf, sum_buf, row_buf,
    dp_send, dp_recv, rs_send, rs_recv, ag_send, ag_recv,
):
    dp, tp = lax.axis_index("dp"), lax.axis_index("tp")
    local = weight_ref.shape[1]
    width = weight_ref.shape[2]
    greet((("dp", n_dp), ("tp", n_tp)))
    mine_buf[...] = gated_ref[...].astype(BF16)
    gathers = []
    for k in range(1, n_dp):
        copy = remote(
            mine_buf, gather_buf.at[k - 1], dp_send.at[k - 1], dp_recv.at[k - 1], "dp",
            lax.rem(dp + k, n_dp),
        )
        copy.start()
        gathers.append(copy)

    per_dp = rows // share

    def product(block, owner):
        part = jnp.dot(block[:, :local], weight_ref[0], preferred_element_type=F32)
        for s in range(per_dp):
            slot = owner * per_dp + s
            part_buf[slot, :, :width] = part[s * share:(s + 1) * share].astype(BF16)
            part_buf[slot, :, width:] = block[s * share:(s + 1) * share, local:]

    product(mine_buf[...], dp)
    for k in range(1, n_dp):
        gathers[k - 1].wait_recv()
        product(gather_buf[k - 1], lax.rem(dp + n_dp - k, n_dp))
    scatters = []
    for k in range(1, n_tp):
        peer = lax.rem(tp + k, n_tp)
        copy = remote(
            part_buf.at[peer], sum_buf.at[k - 1], rs_send.at[k - 1], rs_recv.at[k - 1], "tp", peer
        )
        copy.start()
        scatters.append(copy)
    total = part_buf[tp].astype(F32)
    for k in range(1, n_tp):
        scatters[k - 1].wait_recv()
        total = total + sum_buf[k - 1].astype(F32)
    squares = total[:, width:width + 1] + total[:, width + 1:width + 2]
    update = total[:, :width] * lax.rsqrt(squares / inner + EPS)
    row_buf[tp] = (stream_ref[tp].astype(F32) + update).astype(BF16)
    spreads = []
    for k in range(1, n_tp):
        copy = remote(
            row_buf.at[tp], row_buf.at[tp], ag_send.at[k - 1], ag_recv.at[k - 1], "tp",
            lax.rem(tp + k, n_tp),
        )
        copy.start()
        spreads.append(copy)
    out_ref[tp] = row_buf[tp]
    for k in range(1, n_tp):
        source = lax.rem(tp + n_tp - k, n_tp)
        remote(
            row_buf.at[source], row_buf.at[source], ag_send.at[k - 1], ag_recv.at[k - 1], "tp", source
        ).wait_recv()
        out_ref[source] = row_buf[source]
    for copy in gathers + scatters + spreads:
        copy.wait_send()


def whole(shape):
    return pl.BlockSpec(shape, lambda i: (0,) * len(shape))


def of_layer(shape, layer):
    return pl.BlockSpec((1,) + shape[1:], lambda i: (layer,) + (0,) * (len(shape) - 1))


def project(layer, n_dp, stream, gain, gate, inputs, coupling, steps):
    batch, width = stream.shape
    rows = batch // n_dp
    step_lanes = -(-steps.shape[1] // LANES) * LANES
    columns = gate.shape[2] + inputs.shape[2] + coupling.shape[1] + step_lanes
    return pl.pallas_call(
        functools.partial(project_kernel, n_dp, rows, width * n_dp),
        grid=(1,),
        out_shape=jax.ShapeDtypeStruct((rows, columns), F32),
        in_specs=[
            whole(stream.shape),
            whole(gain.shape),
            of_layer(gate.shape, layer),
            of_layer(inputs.shape, layer),
            whole(coupling.shape),
            of_layer(steps.shape, layer),
        ],
        out_specs=whole((rows, columns)),
        scratch_shapes=[
            pltpu.VMEM((n_dp, rows, columns + LANES), BF16),
            pltpu.VMEM((n_dp - 1, rows, columns + LANES), BF16),
            pltpu.SemaphoreType.DMA((n_dp - 1,)),
            pltpu.SemaphoreType.DMA((n_dp - 1,)),
        ],
        compiler_params=pltpu.CompilerParams(
            collective_id=2 * layer, has_side_effects=True, vmem_limit_bytes=VMEM_LIMIT
        ),
    )(stream, gain, gate, inputs, coupling, steps)


def advance(layer, per_group, drive, decay, write, read, skip, gate, gain, recurrent, held):
    count, inner = drive.shape
    heads = recurrent.shape[2]

    def strip(width):
        return pl.BlockSpec((ROWS, width), lambda i: (i, 0))

    state_spec = pl.BlockSpec(
        (1, ROWS) + recurrent.shape[2:], lambda i: (layer, i, 0, 0, 0)
    )
    in_specs = [
        strip(inner),
        pl.BlockSpec((ROWS, heads, LANES), lambda i: (i, 0, 0)),
        strip(write.shape[1]),
        strip(read.shape[1]),
        strip(inner),
        strip(inner),
        whole(gain.shape),
        state_spec,
    ]
    operands = [drive, decay, write, read, skip, gate, gain, recurrent]
    aliases = {}
    if held is not None:
        aliases = {len(operands): 0}
        operands.append(held)
        in_specs.append(pl.BlockSpec(memory_space=pl.ANY))
    return pl.pallas_call(
        functools.partial(state_kernel, heads, per_group),
        grid=(count // ROWS,),
        out_shape=(
            jax.ShapeDtypeStruct(recurrent.shape, F32),
            jax.ShapeDtypeStruct((count, inner + LANES), F32),
        ),
        in_specs=in_specs,
        out_specs=(state_spec, strip(inner + LANES)),
        input_output_aliases=aliases,
        compiler_params=pltpu.CompilerParams(vmem_limit_bytes=VMEM_LIMIT),
    )(*operands)


def output(layer, n_dp, n_tp, gated, weight, stream):
    rows = gated.shape[0]
    share, width = stream.shape[1:]
    return pl.pallas_call(
        functools.partial(output_kernel, n_dp, n_tp, rows, share, weight.shape[1] * n_tp),
        grid=(1,),
        out_shape=jax.ShapeDtypeStruct(stream.shape, BF16),
        in_specs=[whole(gated.shape), of_layer(weight.shape, layer), whole(stream.shape)],
        out_specs=whole(stream.shape),
        scratch_shapes=[
            pltpu.VMEM(gated.shape, BF16),
            pltpu.VMEM((n_dp - 1,) + gated.shape, BF16),
            pltpu.VMEM((n_tp, share, width + LANES), BF16),
            pltpu.VMEM((n_tp - 1, share, width + LANES), BF16),
            pltpu.VMEM(stream.shape, BF16),
            pltpu.SemaphoreType.DMA((n_dp - 1,)),
            pltpu.SemaphoreType.DMA((n_dp - 1,)),
            pltpu.SemaphoreType.DMA((n_tp - 1,)),
            pltpu.SemaphoreType.DMA((n_tp - 1,)),
            pltpu.SemaphoreType.DMA((n_tp - 1,)),
            pltpu.SemaphoreType.DMA((n_tp - 1,)),
        ],
        compiler_params=pltpu.CompilerParams(
            collective_id=2 * layer + 1, has_side_effects=True, vmem_limit_bytes=VMEM_LIMIT
        ),
    )(gated, weight, stream)


def on_device(
    hidden,
    lengths,
    norm_gain,
    gate_proj,
    input_proj,
    coupling_proj,
    step_proj,
    input_taps,
    coupling_taps,
    step_bias,
    decay_log,
    skip_gain,
    span_bias,
    mix_gain,
    out_proj,
    recurrent,
    input_history,
    coupling_history,
):
    n_dp, n_tp = lax.axis_size("dp"), lax.axis_size("tp")
    batch, width = hidden.shape
    share = batch // n_tp
    rows, heads = recurrent.shape[1:3]
    inner = gate_proj.shape[2]
    groups = coupling_proj.shape[3] // STATE
    per_group = heads // groups
    half = groups * STATE
    steps_t = jnp.swapaxes(step_proj, 1, 2)
    span_index = (lengths - 1) // SPAN_LEN
    onehot = (span_index[:, None] == jnp.arange(SPANS, dtype=jnp.int32)[None, :]).astype(F32)
    stream = hidden.reshape(n_tp, share, width)
    states = None
    inputs_next, couplings_next = [], []
    for l in range(LAYERS):
        coupling = coupling_proj[l].reshape(width, 2 * half)
        sums = project(
            l, n_dp, stream.reshape(batch, width), norm_gain[l:l + 1], gate_proj, input_proj,
            coupling, steps_t,
        )
        gate_in = sums[:, :inner].astype(BF16)
        input_in = sums[:, inner:2 * inner].astype(BF16)
        coupling_in = sums[:, 2 * inner:2 * inner + 2 * half].astype(BF16).reshape(rows, 2, half)
        step_in = head_slice(sums[:, 2 * inner + 2 * half:][:, :step_proj.shape[2]], heads)
        step_in = step_in.astype(BF16)
        input_window = jnp.concatenate([input_history[l], input_in[:, None, :]], axis=1)
        coupling_window = jnp.concatenate([coupling_history[l], coupling_in[:, None]], axis=1)
        inputs_next.append(input_window[:, 1:])
        couplings_next.append(coupling_window[:, 1:])
        input_act = jax.nn.silu(jnp.sum(input_window.astype(F32) * input_taps[l][None], axis=1))
        coupling_act = jax.nn.silu(
            jnp.sum(coupling_window.astype(F32) * coupling_taps[l][None], axis=1)
        )
        span_term = jnp.sum(onehot[:, :, None] * head_slice(span_bias[l], heads)[None], axis=1)
        step_size = jax.nn.softplus(
            step_in.astype(F32) + head_slice(step_bias[l], heads)[None] + span_term
        )
        decay = jnp.exp(-step_size * jnp.exp(head_slice(decay_log[l], heads))[None])
        heads_in = input_act.reshape(rows, heads, HEAD_DIM)
        drive = (step_size[:, :, None] * heads_in).reshape(rows, inner)
        skip = (head_slice(skip_gain[l], heads)[None, :, None] * heads_in).reshape(rows, inner)
        states, gated = advance(
            l,
            per_group,
            drive,
            jnp.broadcast_to(decay[:, :, None], (rows, heads, LANES)),
            coupling_act[:, 0],
            coupling_act[:, 1],
            skip,
            jax.nn.silu(gate_in.astype(F32)),
            mix_gain[l:l + 1],
            recurrent,
            states,
        )
        stream = output(l, n_dp, n_tp, gated, out_proj, stream)
    return (
        stream.reshape(batch, width),
        states,
        jnp.stack(inputs_next),
        jnp.stack(couplings_next),
    )


def solution(mesh):
    placed = (
        P(None, "dp"),
        P("dp"),
        P(None, "dp"),
        P(None, "dp", "tp"),
        P(None, "dp", "tp"),
        P(None, "dp", None, "tp"),
        P(None, "dp", None),
        P(None, None, "tp"),
        P(None, None, None, "tp"),
        P(),
        P(),
        P(),
        P(),
        P(None, "tp"),
        P(None, "tp", "dp"),
        P(None, "dp", "tp", None, None),
        P(None, "dp", None, "tp"),
        P(None, "dp", None, None, "tp"),
    )
    return jax.shard_map(
        on_device,
        mesh=mesh,
        in_specs=placed,
        out_specs=(
            P(None, "dp"),
            P(None, "dp", "tp", None, None),
            P(None, "dp", None, "tp"),
            P(None, "dp", None, None, "tp"),
        ),
        check_vma=False,
    )
```

time: 397 us -> 155 us (0.39)
  blocking collectives: 182 us -> 0 us
  Pallas kernels: 0 us -> 111 us
  waiting for transfers between devices: 96.1 us -> 0 us
  matrix products: 47.1 us -> 0 us
  other arithmetic: 29.2 us -> 8.9 us
  between operations: 15.9 us -> 1.02 us
  local copies, waits for them, and re-layouts: 18.7 us -> 33.5 us
  starting transfers between devices: 7.09 us -> 0 us
    pallas_call x0 -> x6, Pallas kernels: none -> 111 us  [the longest x2 51 us: advance(): pl.pallas_call(functools.partial(state_kernel, heads, per_group), grid=(c...]
    reduce_scatter x6 -> x0, waiting for transfers between devices: 94.7 us -> none  [the longest x2 42.3 us: mixer_layer(): lax.psum_scatter(gate_part.astype(jnp.bfloat16), 'dp', scatter_dimension=...]
    all_gather x4 -> x0, blocking collectives: 72.5 us -> none  [the longest x1 31.2 us: on_device(): lax.all_gather(norm_rows(stream, norm_gain[layer_index + 1]), 'tp', axis=...]
    psum x4 -> x0, blocking collectives: 57.1 us -> none  [the longest x2 42.7 us: mixer_layer(): squares = lax.psum(jnp.sum(gated_out * gated_out, axis=1), 'tp')]
    unnamed x4 -> x0, blocking collectives: 52.6 us -> none
    dot_general x12 -> x0, matrix products: 47.1 us -> none  [the longest x2 32.7 us: mixer_layer(): jnp.einsum('sgrpn,sgn->sgrp', fresh_state, read_vec, precision=lax.Precis...]
    unnamed x42 -> x30, local copies, waits for them, and re-layouts: 3.11 us -> 16.4 us
    another operation x1 -> x2, other arithmetic: 12.1 us -> 0.02 us  [on_device(): jnp.stack(states)]
  transfers between devices with their start and end apart: 10 -> 0, of which waited for: 6 -> 0; matrix products, arithmetic and copies ran while one was open for 9% -> 0% of each run, Pallas kernels for 0% -> 0%
where the time goes in v1:
time: 155 us; the launch traced here: 154 us
  Pallas kernels  111 us (72%)
  local copies, waits for them, and re-layouts  33.5 us (22%)
  other arithmetic  8.9 us (6%)
    pallas_call x2, Pallas kernels, advance(): pl.pallas_call(functools.partial(state_kernel, heads, per_group), grid=(c...  51 us
    pallas_call x2, Pallas kernels, output(): pl.pallas_call(functools.partial(output_kernel, n_dp, n_tp, rows, share,...  45.4 us
    unnamed x30, local copies, waits for them, and re-layouts  16.4 us
    pallas_call x2, Pallas kernels, project(): pl.pallas_call(functools.partial(project_kernel, n_dp, rows, width * n_dp...  14.2 us

profile of v1, /device:TPU:0, one launch (start us, length us, event | category | flops | bytes accessed | tf_op | source)
XLA Modules:
  0.0 154.1 jit_solution(4817000487598909285)
XLA Ops:
  0.6 0.7 and_select_fusion
  1.3 0.8 fusion.33
  2.1 0.8 fusion.34
  2.8 0.1 fusion.17
  2.9 0.6 fusion.21
  3.5 0.8 fusion.32
  4.2 0.1 fusion.20
  4.3 0.1 mul.198
  4.4 0.1 mul.199
  4.4 0.1 mul.221
  4.5 0.1 mul.222
  4.6 0.8 fusion.31
  5.4 0.8 fusion.29
  6.1 0.7 fusion.30
  6.8 0.1 dynamic-slice_bitcast_fusion
  6.9 0.1 multiply_reduce_fusion.5
  7.0 0.1 copy.55
  7.1 0.1 copy.61
  7.2 0.8 fusion.28
  8.0 1.3 slice_bitcast_fusion.10
  9.3 1.6 %slice_bitcast_fusion.1 = (bf16[24,4,512]{2,1,0:T(4,128)(2,1)}, bf16[24,4,512]{2,1,0:T(4,128)(2,1)S(1)}) fusion(bf16[2,24,4,512]{3,2,1,0:T(4,128)(2,1)} %param.34), kind=kLoop, calls=%fused_computation.21 | loop fusion | bytes 393216 | tf_op jit(solution)/shard_map/squeeze | solution.py:351
  11.0 1.1 slice_bitcast_fusion
  12.0 1.7 %reshape.71.stream_ref = bf16[8,12,1024]{2,1,0:T(8,128)(2,1)} reshape(bf16[96,1024]{1,0:T(8,128)(2,1)} %x_ref.1) | data formatting | bytes 393216 | tf_op jit(solution)/shard_map/reshape | solution.py:337
  13.7 2.7 %fusion.25 = (bf16[1,1024,2,256]{3,2,1,0:T(2,128)(2,1)S(1)}, bf16[1,1024,2,256]{3,2,1,0:T(2,128)(2,1)S(1)}) fusion(bf16[2,1024,2,256]{3,2,1,0:T(2,128)(2,1)} %param.23), kind=kLoop, calls=%fused_computation.84 | loop fusion | bytes 4194304 | tf_op jit(solution)/shard_map/slice | solution.py:341
  16.5 0.0 copy-start.3
  16.5 0.0 copy-start.5
  16.5 0.2 copy.70
  16.7 0.2 copy.69
  17.0 1.1 copy-done.3
  18.1 0.6 copy-done.5
  18.7 7.9 %shard_map.201 = f32[24,1664]{1,0:T(8,128)S(1)} custom-call(bf16[96,1024]{1,0:T(8,128)(2,1)S(1)} %copy-done.10, f32[1,1024]{1,0:T(1,128)S(1)} %get-tuple-element.41.gain_ref, bf16[2,1024,512]{2,1,0:T(8,128)(2,1)S(1)} %copy-done.3, bf16[2,1024,512]{2,1,0:T(8,128)(2,1)S(1)} %copy-done.5, bf16[1024,512]{1,0:T(8,128)(2,1)S(1)} %bitcast.62, ...), custom_call_target="tpu_custom_call" | custom-call | tf_op jit(solution)/shard_map/pallas_call | solution.py:213
  26.6 0.1 multiply_exponential_fusion.1
  26.8 0.2 multiply_reduce_fusion.3
  27.0 0.8 fusion.6
  27.9 0.2 multiply_reduce_fusion.1
  28.1 0.8 fusion.5
  28.8 0.1 broadcast_in_dim.9.decay_ref
  28.9 0.1 mul.183
  29.0 0.1 mul.184
  29.2 0.0 copy-start
  29.2 4.6 %copy-done = f32[2,24,8,64,128]{4,3,2,1,0:T(8,128)S(1)} copy-done((f32[2,24,8,64,128]{4,3,2,1,0:T(8,128)S(1)}, f32[2,24,8,64,128]{4,3,2,1,0:T(8,128)}, u32[]{:S(2)}) %copy-start) | copy-done | bytes 12582936
  33.7 25.5 %shard_map.202 = (f32[2,24,8,64,128]{4,3,2,1,0:T(8,128)}, f32[24,640]{1,0:T(8,128)S(1)}) custom-call(f32[24,512]{1,0:T(8,128)S(1)} %get-tuple-element.33.drive_ref, f32[24,8,128]{2,1,0:T(8,128)S(1)} %broadcast_in_dim.9.decay_ref, f32[24,256]{1,0:T(8,128)S(1)} %get-tuple-element.35.write_ref, f32[24,256]{1,0:T(8,128)S(1)} %get-tuple-element.34.read_ref, ...), custom_call_target="tpu_custom_call" | custom-call | tf_op jit(solution)/shard_map/pallas_call | solution.py:264
  59.2 22.9 %shard_map.203.stream_ref = bf16[8,12,1024]{2,1,0:T(8,128)(2,1)S(1)} custom-call(f32[24,640]{1,0:T(8,128)S(1)} %get-tuple-element.8.gated_ref, bf16[2,512,1024]{2,1,0:T(8,128)(2,1)S(1)} %copy-done.2, bf16[8,12,1024]{2,1,0:T(8,128)(2,1)S(1)} %copy-done.9), custom_call_target="tpu_custom_call" | custom-call | tf_op jit(solution)/shard_map/pallas_call | solution.py:281
  82.2 0.7 reshape.72.x_ref
  82.9 1.6 %copy-done.4 = bf16[2,1024,512]{2,1,0:T(8,128)(2,1)S(1)} copy-done((bf16[2,1024,512]{2,1,0:T(8,128)(2,1)S(1)}, bf16[2,1024,512]{2,1,0:T(8,128)(2,1)}, u32[]{:S(2)}) %copy-start.4) | copy-done | bytes 2097176
  84.5 1.6 %copy-done.6 = bf16[2,1024,512]{2,1,0:T(8,128)(2,1)S(1)} copy-done((bf16[2,1024,512]{2,1,0:T(8,128)(2,1)S(1)}, bf16[2,1024,512]{2,1,0:T(8,128)(2,1)}, u32[]{:S(2)}) %copy-start.6) | copy-done | bytes 2097176
  86.1 0.9 copy-done.8
  87.0 0.9 copy-done.11
  88.0 6.3 %shard_map.204 = f32[24,1664]{1,0:T(8,128)S(1)} custom-call(bf16[96,1024]{1,0:T(8,128)(2,1)S(1)} %copy-done.11, f32[1,1024]{1,0:T(1,128)S(1)} %get-tuple-element.40.gain_ref, bf16[2,1024,512]{2,1,0:T(8,128)(2,1)S(1)} %copy-done.4, bf16[2,1024,512]{2,1,0:T(8,128)(2,1)S(1)} %copy-done.6, bf16[1024,512]{1,0:T(8,128)(2,1)S(1)} %bitcast.61, ...), custom_call_target="tpu_custom_call" | custom-call | tf_op jit(solution)/shard_map/pallas_call | solution.py:213
  94.3 0.0 copy-start.12
  94.3 0.1 multiply_exponential_fusion
  94.5 0.9 multiply_reduce_fusion.2
  95.4 0.1 fusion.7
  95.5 1.9 %pad_maximum_fusion.3 = bf16[2,24,4,2,256]{4,3,2,1,0:T(2,128)(2,1)} fusion(bf16[1,24,4,2,256]{4,3,2,1,0:T(2,128)(2,1)S(1)} %fusion.7, bf16[1,24,4,2,256]{4,3,2,1,0:T(2,128)(2,1)} %fusion.6), kind=kLoop, calls=%fused_computation.11 | loop fusion | flops 98304 | bytes 393216 | tf_op jit(solution)/shard_map/stack | solution.py:385
  97.5 1.1 multiply_reduce_fusion
  98.6 1.0 fusion.3
  99.6 0.8 pad_maximum_fusion.2
  100.5 0.1 broadcast_in_dim.11.decay_ref
  100.5 0.1 mul.206
  100.6 0.1 mul.207
  100.8 4.6 %copy-done.1 = f32[2,24,8,64,128]{4,3,2,1,0:T(8,128)S(1)} copy-done((f32[2,24,8,64,128]{4,3,2,1,0:T(8,128)S(1)}, f32[2,24,8,64,128]{4,3,2,1,0:T(8,128)}, u32[]{:S(2)}) %copy-start.1) | copy-done | bytes 12582936
  105.3 25.5 %shard_map.205 = (f32[2,24,8,64,128]{4,3,2,1,0:T(8,128)}, f32[24,640]{1,0:T(8,128)S(1)}) custom-call(f32[24,512]{1,0:T(8,128)S(1)} %get-tuple-element.29.drive_ref, f32[24,8,128]{2,1,0:T(8,128)S(1)} %broadcast_in_dim.11.decay_ref, f32[24,256]{1,0:T(8,128)S(1)} %get-tuple-element.31.write_ref, ...), custom_call_target="tpu_custom_call", output_to_operand_aliasing={{0}: (8, {})} | custom-call | tf_op jit(solution)/shard_map/pallas_call | solution.py:264
  130.8 22.5 %shard_map.206 = bf16[8,12,1024]{2,1,0:T(8,128)(2,1)S(1)} custom-call(f32[24,640]{1,0:T(8,128)S(1)} %get-tuple-element.10.gated_ref, bf16[2,512,1024]{2,1,0:T(8,128)(2,1)S(1)} %copy-done.2, bf16[8,12,1024]{2,1,0:T(8,128)(2,1)S(1)} %shard_map.203.stream_ref), custom_call_target="tpu_custom_call" | custom-call | tf_op jit(solution)/shard_map/pallas_call | solution.py:281
  153.4 0.7 reshape.73
  (36 shorter events, 0.3 us)
Async XLA Ops:
  13.7 3.3 %copy-start.7 = (bf16[2,1024,64]{1,2,0:T(8,128)(2,1)S(1)}, bf16[2,1024,64]{1,2,0:T(8,128)(2,1)}, u32[]{:S(2)}) copy-start(bf16[2,1024,64]{1,2,0:T(8,128)(2,1)} %param.24) | copy-start | bytes 786436
  13.7 3.3 %copy-start.10 = (bf16[96,1024]{1,0:T(8,128)(2,1)S(1)}, bf16[96,1024]{1,0:T(8,128)(2,1)}, u32[]{:S(2)}) copy-start(bf16[96,1024]{1,0:T(8,128)(2,1)} %x_ref.1) | copy-start | bytes 589828
  16.5 1.6 %copy-start.3 = (bf16[2,1024,512]{2,1,0:T(8,128)(2,1)S(1)}, bf16[2,1024,512]{2,1,0:T(8,128)(2,1)}, u32[]{:S(2)}) copy-start(bf16[2,1024,512]{2,1,0:T(8,128)(2,1)} %gate_ref.3) | copy-start | bytes 6291460
  16.5 2.2 %copy-start.5 = (bf16[2,1024,512]{2,1,0:T(8,128)(2,1)S(1)}, bf16[2,1024,512]{2,1,0:T(8,128)(2,1)}, u32[]{:S(2)}) copy-start(bf16[2,1024,512]{2,1,0:T(8,128)(2,1)} %input_ref.3) | copy-start | bytes 6291460
  29.2 4.6 %copy-start = (f32[2,24,8,64,128]{4,3,2,1,0:T(8,128)S(1)}, f32[2,24,8,64,128]{4,3,2,1,0:T(8,128)}, u32[]{:S(2)}) copy-start(f32[2,24,8,64,128]{4,3,2,1,0:T(8,128)} %prior_ref.3) | copy-start | bytes 37748740
  33.7 25.5 %copy-start.2 = (bf16[2,512,1024]{2,1,0:T(8,128)(2,1)S(1)}, bf16[2,512,1024]{2,1,0:T(8,128)(2,1)}, u32[]{:S(2)}) copy-start(bf16[2,512,1024]{2,1,0:T(8,128)(2,1)} %weight_ref.3) | copy-start | bytes 6291460
  33.7 25.5 %copy-start.9 = (bf16[8,12,1024]{2,1,0:T(8,128)(2,1)S(1)}, bf16[8,12,1024]{2,1,0:T(8,128)(2,1)}, u32[]{:S(2)}) copy-start(bf16[8,12,1024]{2,1,0:T(8,128)(2,1)} %reshape.71.stream_ref) | copy-start | bytes 589828
  82.9 1.6 %copy-start.4 = (bf16[2,1024,512]{2,1,0:T(8,128)(2,1)S(1)}, bf16[2,1024,512]{2,1,0:T(8,128)(2,1)}, u32[]{:S(2)}) copy-start(bf16[2,1024,512]{2,1,0:T(8,128)(2,1)} %gate_ref.3) | copy-start | bytes 6291460
  84.5 1.6 %copy-start.6 = (bf16[2,1024,512]{2,1,0:T(8,128)(2,1)S(1)}, bf16[2,1024,512]{2,1,0:T(8,128)(2,1)}, u32[]{:S(2)}) copy-start(bf16[2,1024,512]{2,1,0:T(8,128)(2,1)} %input_ref.3) | copy-start | bytes 6291460
  86.1 0.9 copy-start.8
  87.0 0.9 copy-start.11
  88.0 6.4 %copy-start.13 = (f32[8]{0:T(128)S(1)}, f32[8]{0:T(128)}, u32[]{:S(2)}) copy-start(f32[8]{0:T(128)} %get-tuple-element.59) | copy-start | bytes 100
  94.3 5.4 %copy-start.12 = (bf16[1,24,4,512]{3,2,1,0:T(4,128)(2,1)S(1)}, bf16[1,24,4,512]{3,2,1,0:T(4,128)(2,1)}, u32[]{:S(2)}) copy-start(bf16[1,24,4,512]{3,2,1,0:T(4,128)(2,1)} %fusion.5) | copy-start | bytes 294916
  100.8 4.6 %copy-start.1 = (f32[2,24,8,64,128]{4,3,2,1,0:T(8,128)S(1)}, f32[2,24,8,64,128]{4,3,2,1,0:T(8,128)}, u32[]{:S(2)}) copy-start(f32[2,24,8,64,128]{4,3,2,1,0:T(8,128)} %prior_ref.3) | copy-start | bytes 37748740

commit v2 on v1

--- a/solution.py
+++ b/solution.py
@@ -15,7 +15,7 @@
 LANES = 128
 ROWS = 8
 EPS = 1e-06
-VMEM_LIMIT = 40 * 1024 * 1024
+VMEM_LIMIT = 60 * 1024 * 1024
 MESH = pl.DeviceIdType.MESH
 F32 = jnp.float32
 BF16 = jnp.bfloat16
@@ -59,10 +59,17 @@
 
 
 def project_kernel(
-    n_dp, rows, features, x_ref, gain_ref, gate_ref, input_ref, coup_ref, step_ref,
-    out_ref, send_buf, recv_buf, send_sem, recv_sem,
+    n_dp, rows, features, layer, x_ref, gain_ref, gate_ref, input_ref, coup_ref, step_ref,
+    out_ref, gate_buf, input_buf, coup_buf, send_buf, recv_buf, load_sem, send_sem, recv_sem,
 ):
     me = lax.axis_index("dp")
+    loads = [
+        pltpu.make_async_copy(gate_ref.at[layer], gate_buf, load_sem.at[0]),
+        pltpu.make_async_copy(input_ref.at[layer], input_buf, load_sem.at[1]),
+        pltpu.make_async_copy(coup_ref, coup_buf, load_sem.at[2]),
+    ]
+    for load in loads:
+        load.start()
     greet((("dp", n_dp),))
     values = x_ref[...].astype(F32)
     squares = jnp.sum(values * values, axis=1, keepdims=True)
@@ -73,10 +80,10 @@
             send_buf[d, :, first:first + block.shape[1]] = block[d * rows:(d + 1) * rows].astype(BF16)
 
     first = 0
-    for ref in (gate_ref, input_ref, coup_ref):
-        weight = ref[0] if len(ref.shape) == 3 else ref[...]
-        put(first, jnp.dot(scaled, weight, preferred_element_type=F32))
-        first += weight.shape[1]
+    for load, buf in zip(loads, (gate_buf, input_buf, coup_buf)):
+        load.wait()
+        put(first, jnp.dot(scaled, buf[...], preferred_element_type=F32))
+        first += buf.shape[1]
     steps = lax.dot_general(
         scaled, step_ref[0], (((1,), (1,)), ((), ())), preferred_element_type=F32
     )
@@ -111,18 +118,30 @@
 ):
     fresh_ref, gated_ref = rest[-2], rest[-1]
     drive_t = jnp.transpose(drive_ref[...])
-    lane = lax.broadcasted_iota(jnp.int32, (HEAD_DIM, LANES), 1)
-    sums = [jnp.zeros((HEAD_DIM, LANES), F32) for _ in range(heads)]
-    for j in range(ROWS):
-        for h in range(heads):
-            g = h // per_group
+    groups = heads // per_group
+    lane = lax.broadcasted_iota(jnp.int32, (per_group * HEAD_DIM, LANES), 1)
+    spare = jnp.zeros((LANES - ROWS, STATE), F32)
+    reads = [
+        jnp.transpose(jnp.concatenate([read_ref[:, g * STATE:(g + 1) * STATE], spare], axis=0))
+        for g in range(groups)
+    ]
+    sums = []
+    for g in range(groups):
+        total = jnp.zeros(lane.shape, F32)
+        for j in range(ROWS):
             write = write_ref[j:j + 1, g * STATE:(g + 1) * STATE]
-            read = read_ref[j:j + 1, g * STATE:(g + 1) * STATE]
-            column = drive_t[h * HEAD_DIM:(h + 1) * HEAD_DIM, j:j + 1]
-            fresh = decay_ref[j, h:h + 1, :] * prior_ref[0, j, h] + column * write
-            fresh_ref[0, j, h] = fresh
-            total = jnp.sum(fresh * read, axis=1, keepdims=True)
-            sums[h] = jnp.where(lane == j, total, sums[h])
+            fresh = []
+            for h in range(g * per_group, (g + 1) * per_group):
+                column = drive_t[h * HEAD_DIM:(h + 1) * HEAD_DIM, j:j + 1]
+                block = decay_ref[j, h:h + 1, :] * prior_ref[0, j, h] + column * write
+                fresh_ref[0, j, h] = block
+                fresh.append(block)
+            product = jnp.dot(
+                jnp.concatenate(fresh, axis=0), reads[g],
+                precision=lax.Precision.HIGHEST, preferred_element_type=F32,
+            )
+            total = jnp.where(lane == j, product, total)
+        sums.append(total)
     readout = jnp.transpose(jnp.concatenate(sums, axis=0))[:ROWS]
     gated = (readout + skip_ref[...]) * gate_ref[...]
     squares = jnp.sum(gated * gated, axis=1, keepdims=True)
@@ -132,13 +151,15 @@
 
 
 def output_kernel(
-    n_dp, n_tp, rows, share, inner, gated_ref, weight_ref, stream_ref, out_ref,
-    mine_buf, gather_buf, part_buf, sum_buf, row_buf,
+    n_dp, n_tp, rows, share, inner, layer, gated_ref, weight_ref, stream_ref, out_ref,
+    weight_buf, mine_buf, gather_buf, part_buf, sum_buf, row_buf, load_sem,
     dp_send, dp_recv, rs_send, rs_recv, ag_send, ag_recv,
 ):
     dp, tp = lax.axis_index("dp"), lax.axis_index("tp")
     local = weight_ref.shape[1]
     width = weight_ref.shape[2]
+    load = pltpu.make_async_copy(weight_ref.at[layer], weight_buf, load_sem.at[0])
+    load.start()
     greet((("dp", n_dp), ("tp", n_tp)))
     mine_buf[...] = gated_ref[...].astype(BF16)
     gathers = []
@@ -153,12 +174,13 @@
     per_dp = rows // share
 
     def product(block, owner):
-        part = jnp.dot(block[:, :local], weight_ref[0], preferred_element_type=F32)
+        part = jnp.dot(block[:, :local], weight_buf[...], preferred_element_type=F32)
         for s in range(per_dp):
             slot = owner * per_dp + s
             part_buf[slot, :, :width] = part[s * share:(s + 1) * share].astype(BF16)
             part_buf[slot, :, width:] = block[s * share:(s + 1) * share, local:]
 
+    load.wait()
     product(mine_buf[...], dp)
     for k in range(1, n_dp):
         gathers[k - 1].wait_recv()
@@ -211,21 +233,25 @@
     step_lanes = -(-steps.shape[1] // LANES) * LANES
     columns = gate.shape[2] + inputs.shape[2] + coupling.shape[1] + step_lanes
     return pl.pallas_call(
-        functools.partial(project_kernel, n_dp, rows, width * n_dp),
+        functools.partial(project_kernel, n_dp, rows, width * n_dp, layer),
         grid=(1,),
         out_shape=jax.ShapeDtypeStruct((rows, columns), F32),
         in_specs=[
             whole(stream.shape),
             whole(gain.shape),
-            of_layer(gate.shape, layer),
-            of_layer(inputs.shape, layer),
-            whole(coupling.shape),
+            pl.BlockSpec(memory_space=pl.ANY),
+            pl.BlockSpec(memory_space=pl.ANY),
+            pl.BlockSpec(memory_space=pl.ANY),
             of_layer(steps.shape, layer),
         ],
         out_specs=whole((rows, columns)),
         scratch_shapes=[
+            pltpu.VMEM(gate.shape[1:], BF16),
+            pltpu.VMEM(inputs.shape[1:], BF16),
+            pltpu.VMEM(coupling.shape, BF16),
             pltpu.VMEM((n_dp, rows, columns + LANES), BF16),
             pltpu.VMEM((n_dp - 1, rows, columns + LANES), BF16),
+            pltpu.SemaphoreType.DMA((3,)),
             pltpu.SemaphoreType.DMA((n_dp - 1,)),
             pltpu.SemaphoreType.DMA((n_dp - 1,)),
         ],
@@ -279,17 +305,21 @@
     rows = gated.shape[0]
     share, width = stream.shape[1:]
     return pl.pallas_call(
-        functools.partial(output_kernel, n_dp, n_tp, rows, share, weight.shape[1] * n_tp),
+        functools.partial(output_kernel, n_dp, n_tp, rows, share, weight.shape[1] * n_tp, layer),
         grid=(1,),
         out_shape=jax.ShapeDtypeStruct(stream.shape, BF16),
-        in_specs=[whole(gated.shape), of_layer(weight.shape, layer), whole(stream.shape)],
+        in_specs=[
+            whole(gated.shape), pl.BlockSpec(memory_space=pl.ANY), whole(stream.shape)
+        ],
         out_specs=whole(stream.shape),
         scratch_shapes=[
+            pltpu.VMEM(weight.shape[1:], BF16),
             pltpu.VMEM(gated.shape, BF16),
             pltpu.VMEM((n_dp - 1,) + gated.shape, BF16),
             pltpu.VMEM((n_tp, share, width + LANES), BF16),
             pltpu.VMEM((n_tp - 1, share, width + LANES), BF16),
             pltpu.VMEM(stream.shape, BF16),
+            pltpu.SemaphoreType.DMA((1,)),
             pltpu.SemaphoreType.DMA((n_dp - 1,)),
             pltpu.SemaphoreType.DMA((n_dp - 1,)),
             pltpu.SemaphoreType.DMA((n_tp - 1,)),

time: 155 us -> 121 us (0.78)
  Pallas kernels: 111 us -> 85.8 us
  local copies, waits for them, and re-layouts: 33.5 us -> 24.8 us
    pallas_call x2, Pallas kernels: 51 us -> 18.3 us  [advance(): pl.pallas_call(functools.partial(state_kernel, heads, per_group), grid=(c...]
    unnamed x30 -> x2, local copies, waits for them, and re-layouts: 16.4 us -> 2.4 us
    pallas_call x2, Pallas kernels: 14.2 us -> 19 us  [project(): pl.pallas_call(functools.partial(project_kernel, n_dp, rows, width * n_dp...]
    pallas_call x2, Pallas kernels: 45.4 us -> 48.4 us  [output(): pl.pallas_call(functools.partial(output_kernel, n_dp, n_tp, rows, share,...]
    reshape x2, local copies, waits for them, and re-layouts: 1.45 us -> 3.35 us  [on_device(): stream.reshape(batch, width)]
    another operation x2, other arithmetic: 0.02 us -> 1.85 us
where the time goes in v2:
time: 121 us; the launch traced here: 120 us
  Pallas kernels  85.8 us (71%)
  local copies, waits for them, and re-layouts  24.8 us (20%)
  other arithmetic  8.52 us (7%)
    pallas_call x2, Pallas kernels, output(): pl.pallas_call(functools.partial(output_kernel, n_dp, n_tp, rows, share,...  48.4 us
    pallas_call x2, Pallas kernels, project(): pl.pallas_call(functools.partial(project_kernel, n_dp, rows, width * n_dp...  19 us
    pallas_call x2, Pallas kernels, advance(): pl.pallas_call(functools.partial(state_kernel, heads, per_group), grid=(c...  18.3 us
    reshape x2, local copies, waits for them, and re-layouts, on_device(): stream.reshape(batch, width)  3.35 us
    slice x1, local copies, waits for them, and re-layouts, on_device(): coupling = coupling_proj[l].reshape(width, 2 * half)  2.68 us

profile of v2, /device:TPU:0, one launch (start us, length us, event | category | flops | bytes accessed | tf_op | source)
XLA Modules:
  0.0 119.9 jit_solution(17474225140408615115)
XLA Ops:
  0.6 0.7 and_select_fusion
  1.3 0.8 fusion.33
  2.1 0.8 fusion.34
  2.8 0.1 fusion.17
  2.9 0.1 fusion.21
  3.0 0.8 fusion.32
  3.7 0.1 fusion.20
  3.8 0.1 mul.198
  3.9 0.1 mul.199
  4.0 0.1 mul.221
  4.0 0.1 mul.222
  4.1 1.3 %fusion.31 = (f32[1,512]{1,0:T(1,128)}, f32[1,512]{1,0:T(1,128)}) fusion(f32[2,512]{1,0:T(2,128)} %param.31), kind=kLoop, calls=%fused_computation.90 | loop fusion | bytes 8192 | tf_op jit(solution)/shard_map/slice | solution.py:406
  5.5 1.4 %fusion.29 = (f32[1,1024]{1,0:T(1,128)}, f32[1,1024]{1,0:T(1,128)}) fusion(f32[2,1024]{1,0:T(2,128)} %param.20), kind=kLoop, calls=%fused_computation.88 | loop fusion | bytes 16384 | tf_op jit(solution)/shard_map/slice | solution.py:373
  6.8 0.7 fusion.30
  7.5 0.1 dynamic-slice_bitcast_fusion
  7.6 0.1 multiply_reduce_fusion.5
  7.7 0.1 copy.55
  7.8 0.1 copy.61
  7.8 0.8 fusion.28
  8.7 0.7 slice_bitcast_fusion.10
  9.4 1.0 slice_bitcast_fusion.1
  10.4 1.1 slice_bitcast_fusion
  11.5 1.7 %reshape.71.stream_ref = bf16[8,12,1024]{2,1,0:T(8,128)(2,1)} reshape(bf16[96,1024]{1,0:T(8,128)(2,1)} %x_ref.1) | data formatting | bytes 393216 | tf_op jit(solution)/shard_map/reshape | solution.py:367
  13.2 2.7 %fusion.25 = (bf16[1,1024,2,256]{3,2,1,0:T(2,128)(2,1)S(1)}, bf16[1,1024,2,256]{3,2,1,0:T(2,128)(2,1)S(1)}) fusion(bf16[2,1024,2,256]{3,2,1,0:T(2,128)(2,1)} %param.23), kind=kLoop, calls=%fused_computation.84 | loop fusion | bytes 4194304 | tf_op jit(solution)/shard_map/slice | solution.py:371
  15.9 1.2 copy.70
  17.1 1.2 %copy.69 = bf16[128,8,2,256]{3,1,2,0:T(8,128)(2,1)} copy(bf16[128,8,2,256]{3,2,1,0:T(2,128)(2,1)S(1)} %bitcast.62) | data formatting | bytes 2097152
  18.3 10.5 %shard_map.201 = f32[24,1664]{1,0:T(8,128)} custom-call(bf16[96,1024]{1,0:T(8,128)(2,1)} %x_ref.1, f32[1,1024]{1,0:T(1,128)} %get-tuple-element.41.gain_ref, bf16[2,1024,512]{2,1,0:T(8,128)(2,1)} %gate_ref.3, bf16[2,1024,512]{2,1,0:T(8,128)(2,1)} %input_ref.3, bf16[1024,512]{1,0:T(8,128)(2,1)} %bitcast.64, bf16[2,64,1024]{2,1,0:T(8,128)(2,1)} %bitcast.65), custom_call_target="tpu_custom_call" | custom-call | tf_op jit(solution)/shard_map/pallas_call | solution.py:235
  28.8 0.7 slice.126
  29.5 0.9 convert.10
  30.4 0.1 multiply_exponential_fusion.1
  30.6 0.6 convert_multiply_fusion.1.gate_ref
  31.2 0.2 multiply_reduce_fusion.3
  31.4 0.1 fusion.6
  31.6 0.6 slice_bitcast_fusion.7
  32.2 0.2 multiply_reduce_fusion.1
  32.4 0.1 fusion.5
  32.6 0.7 broadcast_in_dim.9.decay_ref
  33.3 0.1 mul.183
  33.4 0.1 mul.184
  33.5 0.7 broadcast_multiply_fusion.1
  34.1 9.2 %shard_map.202 = (f32[2,24,8,64,128]{4,3,2,1,0:T(8,128)}, f32[24,640]{1,0:T(8,128)}) custom-call(f32[24,512]{1,0:T(8,128)} %get-tuple-element.33.drive_ref, f32[24,8,128]{2,1,0:T(8,128)} %broadcast_in_dim.9.decay_ref, f32[24,256]{1,0:T(8,128)} %get-tuple-element.35.write_ref, f32[24,256]{1,0:T(8,128)} %get-tuple-element.34.read_ref, ...), custom_call_target="tpu_custom_call" | custom-call | tf_op jit(solution)/shard_map/pallas_call | solution.py:290
  43.3 24.2 %shard_map.203.stream_ref = bf16[8,12,1024]{2,1,0:T(8,128)(2,1)} custom-call(f32[24,640]{1,0:T(8,128)} %get-tuple-element.8.gated_ref, bf16[2,512,1024]{2,1,0:T(8,128)(2,1)} %weight_ref.3, bf16[8,12,1024]{2,1,0:T(8,128)(2,1)} %reshape.71.stream_ref), custom_call_target="tpu_custom_call" | custom-call | tf_op jit(solution)/shard_map/pallas_call | solution.py:307
  67.5 1.7 %reshape.72.x_ref = bf16[96,1024]{1,0:T(8,128)(2,1)} reshape(bf16[8,12,1024]{2,1,0:T(8,128)(2,1)} %shard_map.203.stream_ref) | data formatting | bytes 393216 | tf_op jit(solution)/shard_map/reshape | solution.py:373
  69.2 8.5 %shard_map.204 = f32[24,1664]{1,0:T(8,128)} custom-call(bf16[96,1024]{1,0:T(8,128)(2,1)} %reshape.72.x_ref, f32[1,1024]{1,0:T(1,128)} %get-tuple-element.40.gain_ref, bf16[2,1024,512]{2,1,0:T(8,128)(2,1)} %gate_ref.3, bf16[2,1024,512]{2,1,0:T(8,128)(2,1)} %input_ref.3, bf16[1024,512]{1,0:T(8,128)(2,1)} %bitcast.61, bf16[2,64,1024]{2,1,0:T(8,128)(2,1)} %bitcast.66), custom_call_target="tpu_custom_call" | custom-call | tf_op jit(solution)/shard_map/pallas_call | solution.py:235
  77.7 0.7 slice.143
  78.4 0.9 convert.11
  79.3 0.1 multiply_exponential_fusion
  79.5 0.6 convert_multiply_fusion.gate_ref
  80.1 0.2 multiply_reduce_fusion.2
  80.3 0.1 fusion.7
  80.4 1.0 pad_maximum_fusion.3
  81.4 0.6 slice_bitcast_fusion.4
  82.1 0.2 multiply_reduce_fusion
  82.3 0.1 fusion.3
  82.4 0.8 pad_maximum_fusion.2
  83.3 0.7 broadcast_in_dim.11.decay_ref
  84.0 0.1 mul.206
  84.1 0.1 mul.207
  84.2 0.7 broadcast_multiply_fusion
  84.8 9.1 %shard_map.205 = (f32[2,24,8,64,128]{4,3,2,1,0:T(8,128)}, f32[24,640]{1,0:T(8,128)}) custom-call(f32[24,512]{1,0:T(8,128)} %get-tuple-element.29.drive_ref, f32[24,8,128]{2,1,0:T(8,128)} %broadcast_in_dim.11.decay_ref, f32[24,256]{1,0:T(8,128)} %get-tuple-element.31.write_ref, ...), custom_call_target="tpu_custom_call", output_to_operand_aliasing={{0}: (8, {})} | custom-call | tf_op jit(solution)/shard_map/pallas_call | solution.py:290
  94.0 24.2 %shard_map.206 = bf16[8,12,1024]{2,1,0:T(8,128)(2,1)} custom-call(f32[24,640]{1,0:T(8,128)} %get-tuple-element.10.gated_ref, bf16[2,512,1024]{2,1,0:T(8,128)(2,1)} %weight_ref.3, bf16[8,12,1024]{2,1,0:T(8,128)(2,1)} %shard_map.203.stream_ref), custom_call_target="tpu_custom_call" | custom-call | tf_op jit(solution)/shard_map/pallas_call | solution.py:307
  118.2 1.7 %reshape.73 = bf16[96,1024]{1,0:T(8,128)(2,1)} reshape(bf16[8,12,1024]{2,1,0:T(8,128)(2,1)} %shard_map.206) | data formatting | bytes 393216 | tf_op jit(solution)/shard_map/reshape | solution.py:412
  (10 shorter events, 0.2 us)
